TPU v7x, 32 devices: a whole 2x2x4 slice. The times are simulated.
32 devices in a mesh: ep: 8 (over z, x), tp: 4 (over y, core).
Axes of the slice: x: 2, y: 2, z: 4, core: 2. Of those that a mesh axis runs over, the one named last changes fastest.
Arguments:
- query_latent: bfloat16 [1024, 512], P('ep'), may hold values from -6 to 6
- key_latent: bfloat16 [1024, 256], P('ep'), may hold values from -6 to 6
- rope_key: bfloat16 [1024, 64], P('ep'), may hold values from -500 to 500
- query_gain: float32 [512], replicated, may hold values from 0.1 to 1.9
- key_gain: float32 [256], replicated, may hold values from 0.1 to 1.9
- w_query: bfloat16 [512, 1024], P(None, 'tp'), may hold values from -0.25 to 0.25
- w_query_rope: bfloat16 [512, 512], P(None, 'tp'), may hold values from -0.25 to 0.25
- w_key: bfloat16 [256, 1024], P(None, 'tp'), may hold values from -0.375 to 0.375
- w_value: bfloat16 [256, 1024], P(None, 'tp'), may hold values from -0.375 to 0.375
- w_out: bfloat16 [1024, 2048], P('tp'), may hold values from -1.796875 to 1.796875
- tokens_b: bfloat16 [4096, 2048], P('ep'), may hold values from -6 to 6
- ffn_gain: float32 [2048], replicated, may hold values from 0.1 to 1.9
- route_expert: int32 [4096, 2], P('ep'), may hold values from 0 to 7, as said below
- route_weight: float32 [4096, 2], P('ep'), may hold values from 0.2 to 1
- w_gate: bfloat16 [8, 2048, 1024], P('ep', None, 'tp'), may hold values from -0.125 to 0.125
- w_up: bfloat16 [8, 2048, 1024], P('ep', None, 'tp'), may hold values from -0.125 to 0.125
- w_down: bfloat16 [8, 1024, 2048], P('ep', 'tp'), may hold values from -0.1875 to 0.1875
Outputs:
- mixer_out: bfloat16 [1024, 2048], P(('ep', 'tp'))
- moe_out: bfloat16 [4096, 2048], P('ep', 'tp')
Inputs may be any that keep to these rules, and one draw needn't show every extreme that they name: `route_expert`: expert e belongs to group e // 2. A row's 2 experts differ and lie in one group. Among the rows of one device along ep, every group is named by exactly 128 rows and every expert is named exactly 128 times.
All inputs are finite; a program needn't handle non-finite values.
Results may differ from a plain program's by a relative error of at most 0.013.
The roundings to bfloat16 on the way count: a program that leaves them out, or rounds other values in their place, can miss the bound.
Values may be sent and summed in bfloat16 or wider, within the bound.
A program may use at most 64 MiB of HBM per device.

v0:
```python
import math
import jax
import jax.numpy as jnp
from jax import lax
from jax.sharding import PartitionSpec as P

NOPE = 128
ROPE = 64
VDIM = 128
GRID_W = 64
TOPK = 2
epsilon = 1e-06
rotary_base = 10000.0
neg_large = -1e30


def rms_scale(values_in, gain):
    widened = values_in.astype(jnp.float32)
    normed = widened * lax.rsqrt(jnp.mean(widened * widened, axis=-1, keepdims=True) + epsilon)
    return (normed * gain).astype(jnp.bfloat16)


def rotary_tables(positions):
    half_width = ROPE // 2
    inverse = rotary_base ** (-jnp.arange(0, half_width, 2, dtype=jnp.float32) / half_width)
    grid_row = (positions // GRID_W).astype(jnp.float32)
    grid_col = (positions % GRID_W).astype(jnp.float32)
    angle = jnp.concatenate([grid_row[:, None] * inverse, grid_col[:, None] * inverse], axis=-1)
    return (jnp.cos(angle), jnp.sin(angle))


def rotate(values_in, cosine, sine):
    even_part = values_in[..., 0::2]
    odd_part = values_in[..., 1::2]
    turned = jnp.stack(
        [even_part * cosine - odd_part * sine, even_part * sine + odd_part * cosine], axis=-1
    )
    return turned.reshape(values_in.shape)


def fold_blocks(carry, members, step_fn):
    piece_rows = members[0].shape[0]
    block_rows = math.gcd(piece_rows, 1024)
    if block_rows == piece_rows:
        return step_fn(carry, members)
    stacked = tuple(
        (
            member.reshape((piece_rows // block_rows, block_rows) + member.shape[1:])
            for member in members
        )
    )

    def scan_step(inner_carry, blocks):
        return (step_fn(inner_carry, blocks), None)

    result, unused = lax.scan(scan_step, carry, stacked)
    return result


def mixer_half(
    query_latent,
    key_latent,
    rope_key,
    query_gain,
    key_gain,
    w_query,
    w_query_rope,
    w_key,
    w_value,
    w_out,
):
    tok_rows = query_latent.shape[0]
    local_heads = w_query.shape[1] // NOPE
    positions = lax.axis_index("ep") * tok_rows + jnp.arange(tok_rows, dtype=jnp.int32)
    cosine, sine = rotary_tables(positions)
    query_normed = rms_scale(query_latent, query_gain)
    query_nope = jnp.dot(query_normed, w_query, preferred_element_type=jnp.float32).astype(
        jnp.bfloat16
    )
    query_nope = query_nope.reshape(tok_rows, local_heads, NOPE)
    query_rot = jnp.dot(query_normed, w_query_rope, preferred_element_type=jnp.float32)
    query_rot = rotate(
        query_rot.reshape(tok_rows, local_heads, ROPE), cosine[:, None, :], sine[:, None, :]
    )
    query_rot = query_rot.astype(jnp.bfloat16)
    key_rot = rotate(rope_key.astype(jnp.float32), cosine, sine).astype(jnp.bfloat16)
    score_scale = (NOPE + ROPE) ** (-0.5)

    def expand(latent_rows):
        latent_count = latent_rows.shape[0]
        key_normed = rms_scale(latent_rows, key_gain)
        key_nope = jnp.dot(key_normed, w_key, preferred_element_type=jnp.float32).astype(
            jnp.bfloat16
        )
        value_rows = jnp.dot(key_normed, w_value, preferred_element_type=jnp.float32).astype(
            jnp.bfloat16
        )
        return (
            key_nope.reshape(latent_count, local_heads, NOPE),
            value_rows.reshape(latent_count, local_heads, VDIM),
        )

    def attend_block(carry, key_nope, value_rows, key_turn):
        run_max, run_total, run_acc = carry
        scores = jnp.einsum(
            "qhd,khd->hqk", query_nope, key_nope, preferred_element_type=jnp.float32
        )
        scores = scores + jnp.einsum(
            "qhd,kd->hqk", query_rot, key_turn, preferred_element_type=jnp.float32
        )
        scores = scores * score_scale
        new_max = jnp.maximum(run_max, jnp.max(scores, axis=-1))
        correction = jnp.exp(run_max - new_max)
        weights = jnp.exp(scores - new_max[..., None])
        new_total = run_total * correction + jnp.sum(weights, axis=-1)
        added = jnp.einsum(
            "hqk,khd->qhd",
            weights.astype(jnp.bfloat16),
            value_rows,
            preferred_element_type=jnp.float32,
        )
        new_acc = run_acc * jnp.transpose(correction)[..., None] + added
        return (new_max, new_total, new_acc)

    def step_latent(carry, blocks):
        key_nope, value_rows = expand(blocks[0])
        return attend_block(carry, key_nope, value_rows, blocks[1])

    initial = (
        jnp.full((local_heads, tok_rows), neg_large, jnp.float32),
        jnp.zeros((local_heads, tok_rows), jnp.float32),
        jnp.zeros((tok_rows, local_heads, VDIM), jnp.float32),
    )
    final = fold_blocks(
        initial,
        (
            lax.all_gather(key_latent, "ep", axis=0, tiled=True),
            lax.all_gather(key_rot, "ep", axis=0, tiled=True),
        ),
        step_latent,
    )
    run_max, run_total, run_acc = final
    heads_out = (run_acc / jnp.transpose(run_total)[..., None]).astype(jnp.bfloat16)
    heads_out = heads_out.reshape(tok_rows, local_heads * VDIM)
    return lax.psum_scatter(
        jnp.dot(heads_out, w_out, preferred_element_type=jnp.float32).astype(jnp.bfloat16),
        "tp",
        scatter_dimension=0,
        tiled=True,
    )


def expert_half(tokens_b, ffn_gain, route_expert, route_weight, w_gate, w_up, w_down):
    tok_rows = tokens_b.shape[0]
    expert_count = lax.axis_size("ep")
    capacity = TOPK * tok_rows // expert_count
    normed = rms_scale(tokens_b, ffn_gain)
    copies = route_expert.reshape(tok_rows * TOPK)
    chosen = (copies[:, None] == jnp.arange(expert_count, dtype=jnp.int32)[None, :]).astype(
        jnp.int32
    )
    earlier = jnp.cumsum(chosen, axis=0) - chosen
    slot_index = jnp.sum(earlier * chosen, axis=1)
    target = copies * capacity + slot_index
    source_row = (
        jnp.zeros((expert_count * capacity,), jnp.int32)
        .at[target]
        .set(jnp.arange(tok_rows * TOPK, dtype=jnp.int32) // TOPK)
    )
    outgoing = jnp.take(normed, source_row, axis=0)
    share_cols = outgoing.shape[1] // lax.axis_size("tp")
    own_cols = lax.dynamic_slice_in_dim(outgoing, lax.axis_index("tp") * share_cols, share_cols, 1)
    arrived = lax.all_to_all(own_cols, "ep", split_axis=0, concat_axis=0, tiled=True)
    member = lax.all_gather(arrived, "tp", axis=1, tiled=True)
    gate_rows = w_gate[0]
    up_rows = w_up[0]
    gate_act = jnp.dot(member, gate_rows, preferred_element_type=jnp.float32)
    up_act = jnp.dot(member, up_rows, preferred_element_type=jnp.float32)
    hidden = (jax.nn.silu(gate_act) * up_act).astype(jnp.bfloat16)
    partial_term = jnp.dot(hidden, w_down[0], preferred_element_type=jnp.float32)
    shared = lax.psum_scatter(
        partial_term.astype(jnp.bfloat16), "tp", scatter_dimension=1, tiled=True
    )
    returned = lax.all_to_all(shared, "ep", split_axis=0, concat_axis=0, tiled=True)
    picked = (
        jnp.take(returned, target, axis=0)
        .astype(jnp.float32)
        .reshape(tok_rows, TOPK, returned.shape[1])
    )
    combined = jnp.sum(picked * route_weight[:, :, None], axis=1)
    return combined.astype(jnp.bfloat16)


def body(
    query_latent,
    key_latent,
    rope_key,
    query_gain,
    key_gain,
    w_query,
    w_query_rope,
    w_key,
    w_value,
    w_out,
    tokens_b,
    ffn_gain,
    route_expert,
    route_weight,
    w_gate,
    w_up,
    w_down,
):
    mixer_out = mixer_half(
        query_latent,
        key_latent,
        rope_key,
        query_gain,
        key_gain,
        w_query,
        w_query_rope,
        w_key,
        w_value,
        w_out,
    )
    moe_out = expert_half(tokens_b, ffn_gain, route_expert, route_weight, w_gate, w_up, w_down)
    return (mixer_out, moe_out)


def solution(mesh):
    in_specs = (
        P("ep", None),
        P("ep", None),
        P("ep", None),
        P(),
        P(),
        P(None, "tp"),
        P(None, "tp"),
        P(None, "tp"),
        P(None, "tp"),
        P("tp", None),
        P("ep", None),
        P(),
        P("ep", None),
        P("ep", None),
        P("ep", None, "tp"),
        P("ep", None, "tp"),
        P("ep", "tp", None),
    )
    out_specs = (P(("ep", "tp"), None), P("ep", "tp"))
    return jax.shard_map(body, mesh=mesh, in_specs=in_specs, out_specs=out_specs, check_vma=False)
```

profile of v0, /device:TPU:0, one launch (start us, length us, event | category | flops | bytes accessed | tf_op | source)
XLA Modules:
  0.0 206.5 jit_solution(17284445992472675687)
XLA Ops:
  7.2 0.9 copy.40
  8.5 0.7 broadcast_multiply_fusion.2
  9.2 2.3 %reduce-window.6 = s32[8,8,128]{2,1,0:T(8,128)S(1)} reduce-window(s32[8,8,128]{2,1,0:T(8,128)S(1)} %fusion.43, s32[]{:T(128)} %constant.106.clone.1), window={size=1x1x128 pad=0_0x0_0x127_0}, to_apply=%region_5.6 | reduce-window | flops 1040384 | bytes 65540 | tf_op jit(solution)/shard_map/reduce-window
  11.5 0.3 slice_reduce_fusion
  12.4 4.3 %scatter_custom_fusion = s32[1024]{0:T(1024)S(1)} fusion(s32[1024]{0:T(1024)S(1)} %bitcast.101, s32[1024]{0:T(1024)S(1)} %add_select_fusion, s32[]{:T(128)} %constant.106.clone.1), kind=kCustom, calls=%fused_computation.95 | custom fusion | bytes 4100 | tf_op jit(solution)/shard_map/scatter | solution.py:168
  16.7 2.1 %fusion = f32[512]{0:T(512)S(1)} fusion(bf16[512,2048]{1,0:T(8,128)(2,1)} %param.27), kind=kLoop, calls=%fused_computation.5 | loop fusion | flops 3145216 | bytes 2099200 | tf_op jit(solution)/shard_map/reduce_sum | solution.py:19
  18.8 2.1 %fusion.2 = bf16[512,2048]{1,0:T(8,128)(2,1)S(1)} fusion(bf16[512,2048]{1,0:T(8,128)(2,1)} %param.27, f32[2048]{0:T(1024)} %param.28, f32[512]{0:T(512)S(1)} %add_rsqrt_fusion.1), kind=kLoop, calls=%fused_computation.7 | loop fusion | flops 4194304 | bytes 4204544 | tf_op jit(solution)/shard_map/convert_element_type | solution.py:20
  20.9 6.0 %gather_fusion = bf16[1024,2048]{1,0:T(8,128)(2,1)} fusion(bf16[512,2048]{1,0:T(8,128)(2,1)S(1)} %fusion.2, s32[1024]{0:T(1024)S(1)} %fusion.53), kind=kCustom, calls=%fused_computation | custom fusion | bytes 8392704 | tf_op jit(solution)/shard_map/jit(_take)/gather | solution.py:170
  27.0 1.6 dynamic-slice_select_fusion
  28.6 32.9 %all_to_all.24 = bf16[8,128,512]{2,1,0:T(8,128)(2,1)} all-to-all(bf16[8,128,512]{2,1,0:T(8,128)(2,1)S(1)} %bitcast.92), channel_id=1, replica_groups=mesh['ep'=8,'tp'=4] {'ep'}, dimensions={0} | all-to-all | bytes 2097152 | tf_op jit(solution)/shard_map/all_to_all | solution.py:173
  61.6 33.6 %all-gather.2.cloned.1.call-done = bf16[1024,2048]{1,0:T(8,128)(2,1)} async-done(((bf16[1024,512]{1,0:T(8,128)(2,1)}), bf16[1024,2048]{1,0:T(8,128)(2,1)}) %all-gather.2.cloned.1.call-update) | async-done | bytes 4194320 | tf_op jit(solution)/shard_map/all_gather | solution.py:174
  95.2 4.5 %fusion.16 = f32[1024,256]{1,0:T(8,128)} fusion(bf16[1024,2048]{1,0:T(8,128)(2,1)} %all-gather.2.cloned.1.call-done, bf16[1,2048,256]{2,1,0:T(8,128)(2,1)S(1)} %copy-done.11), kind=kOutput, calls=%fused_computation.33 | convolution fusion | flops 1073741824 | bytes 6291456 | tf_op jit(solution)/shard_map/dot_general | solution.py:177
  99.8 8.8 %convolution_convert_fusion = bf16[1024,2048]{1,0:T(8,128)(2,1)} fusion(bf16[1024,2048]{1,0:T(8,128)(2,1)} %all-gather.2.cloned.1.call-done, bf16[1,256,2048]{2,1,0:T(8,128)(2,1)S(1)} %copy-done, bf16[1,2048,256]{2,1,0:T(8,128)(2,1)S(1)} %copy-done.12, f32[1024,256]{1,0:T(8,128)} %fusion.16), kind=kOutput, calls=%fused_computation.8 | convolution fusion | flops 2151153664 | bytes 11534336 | tf_op jit(solution)/shard_map/dot_general | solution.py:180
  108.6 0.6 copy-done.7
  109.6 0.3 fusion.37
  110.2 26.2 %all_gather.10 = bf16[1024,64]{0,1:T(8,128)(2,1)S(1)} all-gather(bf16[128,64]{0,1:T(8,128)(2,1)S(1)} %bitcast.99), channel_id=1, replica_groups=mesh['ep'=8,'tp'=4] {'ep'}, dimensions={0}, use_global_device_ids=true | all-gather | bytes 147456 | tf_op jit(solution)/shard_map/all_gather | solution.py:138
  136.4 0.2 fusion.9
  136.7 31.4 %all_gather.9 = bf16[1024,256]{1,0:T(8,128)(2,1)S(1)} all-gather(bf16[128,256]{1,0:T(8,128)(2,1)S(1)} %copy-done.6), channel_id=1, replica_groups=mesh['ep'=8,'tp'=4] {'ep'}, dimensions={0}, use_global_device_ids=true | all-gather | bytes 589824 | tf_op jit(solution)/shard_map/all_gather | solution.py:137
  168.1 0.2 fusion.10
  168.3 0.5 convolution_convert_fusion.3
  168.8 0.3 fusion.34
  169.1 0.4 fusion.59
  169.6 4.3 %all-to-all-start.1 = ((bf16[8,128,512]{2,1,0:T(8,128)(2,1)}), bf16[8,128,512]{2,1,0:T(8,128)(2,1)S(1)}, u32[]{:S(2)}, u32[]{:S(2)}) async-start(bf16[8,128,512]{2,1,0:T(8,128)(2,1)} %bitcast.93), calls=%async_computation.3 | async-start | bytes 2097152 | tf_op jit(solution)/shard_map/all_to_all | solution.py:184
  173.9 0.2 reduce-scatter.3.cloned.1.call-start
  174.2 0.3 fusion.23
  174.5 1.5 convolution_convert_fusion.2
  176.1 0.4 fusion.8
  176.5 1.2 convolution_convert_fusion.1
  178.4 12.0 %all-to-all-done.1 = bf16[8,128,512]{2,1,0:T(8,128)(2,1)S(1)} async-done(((bf16[8,128,512]{2,1,0:T(8,128)(2,1)}), bf16[8,128,512]{2,1,0:T(8,128)(2,1)S(1)}, u32[]{:S(2)}, u32[]{:S(2)}) %all-to-all-start.1) | async-done | bytes 1048608 | tf_op jit(solution)/shard_map/all_to_all | solution.py:184
  190.3 4.0 %gather_fusion.1 = bf16[1024,512]{1,0:T(8,128)(2,1)S(1)} fusion(bf16[1024,512]{1,0:T(8,128)(2,1)S(1)} %bitcast.90, s32[1024]{0:T(1024)S(1)} %broadcast_clamp_fusion), kind=kCustom, calls=%fused_computation.1 | custom fusion | bytes 2101248 | tf_op jit(solution)/shard_map/jit(_take)/gather | solution.py:186
  194.3 0.4 gather.12
  194.7 5.2 %multiply_reduce_fusion = bf16[512,512]{1,0:T(8,128)(2,1)} fusion(bf16[512,2,512]{2,1,0:T(2,128)(2,1)S(1)} %gather.12, pred[512,2]{1,0:T(8,128)(4,1)S(1)} %copy.43, f32[512,2]{1,0:T(8,128)S(1)} %copy.45), kind=kLoop, calls=%fused_computation.10 | loop fusion | flops 1835008 | bytes 1577984 | tf_op jit(solution)/shard_map/reduce_sum | solution.py:190
  (75 shorter events, 2.5 us)
Async XLA Ops:
  7.2 92.6 %copy-start = (bf16[1,256,2048]{2,1,0:T(8,128)(2,1)S(1)}, bf16[1,256,2048]{2,1,0:T(8,128)(2,1)}, u32[]{:S(2)}) copy-start(bf16[1,256,2048]{2,1,0:T(8,128)(2,1)} %param.33) | copy-start | bytes 3145732
  7.2 88.1 %all-gather.2.cloned.1.call-start = ((), (), s32[]{:S(2)}) async-start(), calls=%async_computation.5 | async-start | bytes 5242880 | tf_op jit(solution)/shard_map/all_gather | solution.py:174
  27.0 68.3 %copy-start.11 = (bf16[1,2048,256]{2,1,0:T(8,128)(2,1)S(1)}, bf16[1,2048,256]{2,1,0:T(8,128)(2,1)}, u32[]{:S(2)}) copy-start(bf16[1,2048,256]{2,1,0:T(8,128)(2,1)} %param.31) | copy-start | bytes 3145732
  61.6 38.2 %copy-start.12 = (bf16[1,2048,256]{2,1,0:T(8,128)(2,1)S(1)}, bf16[1,2048,256]{2,1,0:T(8,128)(2,1)}, u32[]{:S(2)}) copy-start(bf16[1,2048,256]{2,1,0:T(8,128)(2,1)} %param.32) | copy-start | bytes 3145732
  61.6 108.0 %reduce-scatter.5.cloned.1.call-start = ((), (), s32[]{:S(2)}) async-start(), calls=%async_computation.6 | async-start | bytes 5242880 | tf_op jit(solution)/shard_map/reduce_scatter | solution.py:181
  108.6 0.7 copy-start.7
  108.6 0.9 copy-start.2
  108.6 1.0 copy-start.5
  108.6 1.0 copy-start.9
  108.6 27.9 %copy-start.4 = (bf16[512,256]{1,0:T(8,128)(2,1)S(1)}, bf16[512,256]{1,0:T(8,128)(2,1)}, u32[]{:S(2)}) copy-start(bf16[512,256]{1,0:T(8,128)(2,1)} %param.22) | copy-start | bytes 786436
  108.6 28.1 %copy-start.6 = (bf16[128,256]{1,0:T(8,128)(2,1)S(1)}, bf16[128,256]{1,0:T(8,128)(2,1)}, u32[]{:S(2)}) copy-start(bf16[128,256]{1,0:T(8,128)(2,1)} %param.18) | copy-start | bytes 196612
  108.6 59.7 %copy-start.13 = (bf16[256,256]{1,0:T(8,128)(2,1)S(1)}, bf16[256,256]{1,0:T(8,128)(2,1)}, u32[]{:S(2)}) copy-start(bf16[256,256]{1,0:T(8,128)(2,1)} %param.24) | copy-start | bytes 393220
  108.6 59.7 %copy-start.15 = (f32[256]{0:T(256)S(1)}, f32[256]{0:T(256)}, u32[]{:S(2)}) copy-start(f32[256]{0:T(256)} %param.21) | copy-start | bytes 3076
  168.1 1.1 copy-start.1
  168.3 6.2 %copy-start.14 = (bf16[256,256]{1,0:T(8,128)(2,1)S(1)}, bf16[256,256]{1,0:T(8,128)(2,1)}, u32[]{:S(2)}) copy-start(bf16[256,256]{1,0:T(8,128)(2,1)} %param.25) | copy-start | bytes 393220
  169.6 8.4 %copy-start.8 = (s32[512,2]{0,1:T(2,128)S(1)}, s32[512,2]{0,1:T(2,128)}, u32[]{:S(2)}) copy-start(s32[512,2]{0,1:T(2,128)} %param.29) | copy-start | bytes 12292
  169.6 8.6 %copy-start.10 = (f32[512,2]{0,1:T(2,128)S(1)}, f32[512,2]{0,1:T(2,128)}, u32[]{:S(2)}) copy-start(f32[512,2]{0,1:T(2,128)} %param.30) | copy-start | bytes 12292
  169.6 20.7 %all-to-all-start.1 = ((bf16[8,128,512]{2,1,0:T(8,128)(2,1)}), bf16[8,128,512]{2,1,0:T(8,128)(2,1)S(1)}, u32[]{:S(2)}, u32[]{:S(2)}) async-start(bf16[8,128,512]{2,1,0:T(8,128)(2,1)} %bitcast.93), calls=%async_computation.3 | async-start | bytes 2097152 | tf_op jit(solution)/shard_map/all_to_all | solution.py:184
  173.9 26.0 %reduce-scatter.3.cloned.1.call-start = ((), (), s32[]{:S(2)}) async-start(), calls=%async_computation.4 | async-start | bytes 655360 | tf_op jit(solution)/shard_map/reduce_scatter | solution.py:145
  174.2 2.3 %copy-start.3 = (bf16[256,2048]{1,0:T(8,128)(2,1)S(1)}, bf16[256,2048]{1,0:T(8,128)(2,1)}, u32[]{:S(2)}) copy-start(bf16[256,2048]{1,0:T(8,128)(2,1)} %param.26) | copy-start | bytes 3145732
Sparse Core Ops, SparseCore 0:
  61.7 33.4 all-gather.1
  108.8 44.3 reduce-scatter.4
  177.8 22.1 reduce-scatter.2
where the time goes:
time: 207 us; the launch traced here: 206 us
  blocking collectives  90.5 us (44%)
  waiting for transfers between devices  45.7 us (22%)
  local copies, waits for them, and re-layouts  18.2 us (9%)
  matrix products  18.1 us (9%)
  other arithmetic  15.2 us (7%)
  between operations  14.2 us (7%)
  starting transfers between devices  4.65 us (2%)
    all_gather x1, waiting for transfers between devices, expert_half(): member = lax.all_gather(arrived, 'tp', axis=1, tiled=True)  33.6 us
    all_to_all x1, blocking collectives, expert_half(): lax.all_to_all(own_cols, 'ep', split_axis=0, concat_axis=0, tiled=True)  32.9 us
    all_gather x1, blocking collectives, mixer_half(): lax.all_gather(key_latent, 'ep', axis=0, tiled=True)  31.4 us
    all_gather x1, blocking collectives, mixer_half(): lax.all_gather(key_rot, 'ep', axis=0, tiled=True)  26.2 us
    all_to_all x1, waiting for transfers between devices, expert_half(): lax.all_to_all(shared, 'ep', split_axis=0, concat_axis=0, tiled=True)  12 us
    dot_general x1, matrix products, expert_half(): jnp.dot(hidden, w_down[0], preferred_element_type=jnp.float32)  8.8 us
    gather x1, local copies, waits for them, and re-layouts, expert_half(): outgoing = jnp.take(normed, source_row, axis=0)  6.02 us
    reduce_sum x1, other arithmetic, expert_half(): combined = jnp.sum(picked * route_weight[:, :, None], axis=1)  5.21 us
  transfers between devices with their start and end apart: 4, of which 2 were waited for; matrix products, arithmetic and copies ran while one was open for 8% of the time, Pallas kernels for 0%

commit v1 on v0

--- a/solution.py
+++ b/solution.py
@@ -3,6 +3,7 @@
 import jax.numpy as jnp
 from jax import lax
 from jax.sharding import PartitionSpec as P
+from jax.lax import axis_index, axis_size, ppermute
 
 NOPE = 128
 ROPE = 64
@@ -171,7 +172,25 @@
     share_cols = outgoing.shape[1] // lax.axis_size("tp")
     own_cols = lax.dynamic_slice_in_dim(outgoing, lax.axis_index("tp") * share_cols, share_cols, 1)
     arrived = lax.all_to_all(own_cols, "ep", split_axis=0, concat_axis=0, tiled=True)
-    member = lax.all_gather(arrived, "tp", axis=1, tiled=True)
+
+    def _pass_things(v0):
+        axis_name = "tp"
+        how_many = axis_size(axis_name)
+        left_arr = range(how_many)
+        steps_seen = list(map(lambda tick: (tick, (tick + 1) % how_many), left_arr))
+
+        def extend_matrix(vec_out):
+            if len(vec_out) == how_many:
+                return vec_out
+            return extend_matrix(
+                [ppermute(vec_out[0], axis_name=axis_name, perm=steps_seen), *vec_out]
+            )
+
+        extra = extend_matrix([v0])
+        base_arr = jnp.concatenate(extra, axis=1)
+        return jnp.roll(base_arr, (axis_index(axis_name) + 1) * v0.shape[1], axis=1)
+
+    member = _pass_things(arrived)
     gate_rows = w_gate[0]
     up_rows = w_up[0]
     gate_act = jnp.dot(member, gate_rows, preferred_element_type=jnp.float32)

time: 207 us -> 224 us (1.082)
  waiting for transfers between devices: 45.7 us -> 55.8 us
  local copies, waits for them, and re-layouts: 18.2 us -> 26.8 us
    ppermute x0 -> x3, waiting for transfers between devices: none -> 43.1 us  [extend_matrix(): ppermute(vec_out[0], axis_name=axis_name, perm=steps_seen)]
    all_gather x1 -> x0, waiting for transfers between devices: 33.6 us -> none  [expert_half(): member = lax.all_gather(arrived, 'tp', axis=1, tiled=True)]
    unnamed x34 -> x39, local copies, waits for them, and re-layouts: 1.93 us -> 10.3 us
    dot_general x1, matrix products: 4.51 us -> 1.26 us  [expert_half(): up_act = jnp.dot(member, up_rows, preferred_element_type=jnp.float32)]
  transfers between devices with their start and end apart: 4 -> 6, of which waited for: 2 -> 5; matrix products, arithmetic and copies ran while one was open for 8% -> 8% of each run, Pallas kernels for 0% -> 0%
where the time goes in v1:
time: 224 us; the launch traced here: 223 us
  blocking collectives  90.9 us (41%)
  waiting for transfers between devices  55.8 us (25%)
  local copies, waits for them, and re-layouts  26.8 us (12%)
  matrix products  16.2 us (7%)
  other arithmetic  15.1 us (7%)
  between operations  14.6 us (7%)
  starting transfers between devices  3.84 us (2%)
    ppermute x3, waiting for transfers between devices, extend_matrix(): ppermute(vec_out[0], axis_name=axis_name, perm=steps_seen)  43.1 us
    all_to_all x1, blocking collectives, expert_half(): lax.all_to_all(own_cols, 'ep', split_axis=0, concat_axis=0, tiled=True)  32.8 us
    all_gather x1, blocking collectives, mixer_half(): lax.all_gather(key_latent, 'ep', axis=0, tiled=True)  31.9 us
    all_gather x1, blocking collectives, mixer_half(): lax.all_gather(key_rot, 'ep', axis=0, tiled=True)  26.1 us
    all_to_all x1, waiting for transfers between devices, expert_half(): lax.all_to_all(shared, 'ep', split_axis=0, concat_axis=0, tiled=True)  10.7 us
    unnamed x39, local copies, waits for them, and re-layouts  10.3 us
    dot_general x1, matrix products, expert_half(): jnp.dot(hidden, w_down[0], preferred_element_type=jnp.float32)  8.94 us
    gather x1, local copies, waits for them, and re-layouts, expert_half(): outgoing = jnp.take(normed, source_row, axis=0)  6.02 us
  transfers between devices with their start and end apart: 6, of which 5 were waited for; matrix products, arithmetic and copies ran while one was open for 8% of the time, Pallas kernels for 0%

profile of v1, /device:TPU:0, one launch (start us, length us, event | category | flops | bytes accessed | tf_op | source)
XLA Modules:
  0.0 223.2 jit_solution(12602436825409407142)
XLA Ops:
  7.2 0.9 copy.40
  8.5 0.7 broadcast_multiply_fusion.2
  9.2 2.3 %reduce-window.6 = s32[8,8,128]{2,1,0:T(8,128)S(1)} reduce-window(s32[8,8,128]{2,1,0:T(8,128)S(1)} %fusion.47, s32[]{:T(128)} %constant.125.clone.1), window={size=1x1x128 pad=0_0x0_0x127_0}, to_apply=%region_5.6 | reduce-window | flops 1040384 | bytes 65540 | tf_op jit(solution)/shard_map/reduce-window
  12.4 4.3 %scatter_custom_fusion = s32[1024]{0:T(1024)S(1)} fusion(s32[1024]{0:T(1024)S(1)} %bitcast.104, s32[1024]{0:T(1024)S(1)} %add_select_fusion, s32[]{:T(128)} %constant.125.clone.1), kind=kCustom, calls=%fused_computation.100 | custom fusion | bytes 4100 | tf_op jit(solution)/shard_map/scatter | solution.py:169
  16.7 2.1 fusion
  18.8 2.1 fusion.2
  20.9 6.0 %gather_fusion = bf16[1024,2048]{1,0:T(8,128)(2,1)} fusion(bf16[512,2048]{1,0:T(8,128)(2,1)S(1)} %fusion.2, s32[1024]{0:T(1024)S(1)} %fusion.57), kind=kCustom, calls=%fused_computation | custom fusion | bytes 8392704 | tf_op jit(solution)/shard_map/jit(_take)/gather | solution.py:171
  27.0 1.5 dynamic-slice_select_fusion
  28.5 32.8 %all_to_all.24 = bf16[8,128,512]{2,1,0:T(8,128)(2,1)S(1)} all-to-all(bf16[8,128,512]{2,1,0:T(8,128)(2,1)S(1)} %bitcast.95), channel_id=1, replica_groups=mesh['ep'=8,'tp'=4] {'ep'}, dimensions={0} | all-to-all | bytes 2097152 | tf_op jit(solution)/shard_map/all_to_all | solution.py:174
  61.4 14.2 %collective-permute-done = bf16[1024,512]{1,0:T(8,128)(2,1)S(1)} collective-permute-done((bf16[1024,512]{1,0:T(8,128)(2,1)S(1)}, bf16[1024,512]{1,0:T(8,128)(2,1)S(1)}, u32[]{:S(2)}, u32[]{:S(2)}) %collective-permute-start) | collective-permute-done | bytes 1048608 | tf_op jit(solution)/shard_map/ppermute | solution.py:186
  75.6 14.3 %collective-permute-done.1 = bf16[1024,512]{1,0:T(8,128)(2,1)} collective-permute-done((bf16[1024,512]{1,0:T(8,128)(2,1)S(1)}, bf16[1024,512]{1,0:T(8,128)(2,1)}, u32[]{:S(2)}, u32[]{:S(2)}) %collective-permute-start.1) | collective-permute-done | bytes 1048608 | tf_op jit(solution)/shard_map/ppermute | solution.py:186
  89.9 14.5 %collective-permute-done.2 = bf16[1024,512]{1,0:T(8,128)(2,1)} collective-permute-done((bf16[1024,512]{1,0:T(8,128)(2,1)}, bf16[1024,512]{1,0:T(8,128)(2,1)}, u32[]{:S(2)}, u32[]{:S(2)}) %collective-permute-start.2) | collective-permute-done | bytes 1048608 | tf_op jit(solution)/shard_map/ppermute | solution.py:186
  104.5 1.4 constant_dynamic-update-slice_fusion.7
  105.8 1.4 constant_dynamic-update-slice_fusion.6
  107.5 1.4 constant_dynamic-update-slice_fusion.3
  108.9 1.4 constant_dynamic-update-slice_fusion.2
  110.6 3.2 %copy-done.5 = bf16[1024,4096]{1,0:T(8,128)(2,1)} copy-done((bf16[1024,4096]{1,0:T(8,128)(2,1)}, bf16[1024,4096]{1,0:T(8,128)(2,1)S(1)}, u32[]{:S(2)}) %copy-start.5) | copy-done | bytes 8388632
  113.9 1.3 fusion.3
  115.2 8.9 %convolution_convert_fusion = bf16[1024,2048]{1,0:T(8,128)(2,1)} fusion(bf16[1,256,2048]{2,1,0:T(8,128)(2,1)S(1)} %copy-done, f32[1024,256]{1,0:T(8,128)S(1)} %fusion.3, bf16[1024,4096]{1,0:T(8,128)(2,1)} %copy-done.5, s32[]{:T(128)S(6)} %select_n.79, bf16[1,2048,256]{2,1,0:T(8,128)(2,1)} %param.31), kind=kOutput, calls=%fused_computation.8 | convolution fusion | flops 2151153664 | bytes 11534340 | tf_op jit(solution)/shard_map/dot_general | solution.py:199
  125.1 26.1 %all_gather.7 = bf16[1024,64]{0,1:T(8,128)(2,1)S(1)} all-gather(bf16[128,64]{0,1:T(8,128)(2,1)S(1)} %bitcast.102), channel_id=1, replica_groups=mesh['ep'=8,'tp'=4] {'ep'}, dimensions={0}, use_global_device_ids=true | all-gather | bytes 147456 | tf_op jit(solution)/shard_map/all_gather | solution.py:139
  151.4 31.9 %all_gather.6 = bf16[1024,256]{1,0:T(8,128)(2,1)S(1)} all-gather(bf16[128,256]{1,0:T(8,128)(2,1)S(1)} %copy-done.6), channel_id=1, replica_groups=mesh['ep'=8,'tp'=4] {'ep'}, dimensions={0}, use_global_device_ids=true | all-gather | bytes 589824 | tf_op jit(solution)/shard_map/all_gather | solution.py:138
  183.6 0.5 convolution_convert_fusion.3
  184.4 0.4 fusion.66
  184.9 3.6 %all-to-all-start.1 = ((bf16[8,128,512]{2,1,0:T(8,128)(2,1)}), bf16[8,128,512]{2,1,0:T(8,128)(2,1)S(1)}, u32[]{:S(2)}, u32[]{:S(2)}) async-start(bf16[8,128,512]{2,1,0:T(8,128)(2,1)} %bitcast.96), calls=%async_computation.3 | async-start | bytes 2097152 | tf_op jit(solution)/shard_map/all_to_all | solution.py:203
  189.0 1.5 convolution_convert_fusion.2
  190.5 0.4 fusion.11
  190.9 2.4 %convolution_convert_fusion.1 = bf16[128,2048]{1,0:T(8,128)(2,1)} fusion(bf16[128,256]{0,1:T(8,128)(2,1)S(1)} %bitcast.101, bf16[256,2048]{1,0:T(8,128)(2,1)} %param.26), kind=kOutput, calls=%fused_computation.13 | convolution fusion | flops 134479872 | bytes 1638400 | tf_op jit(solution)/shard_map/dot_general | solution.py:147
  194.1 10.7 %all-to-all-done.1 = bf16[8,128,512]{2,1,0:T(8,128)(2,1)S(1)} async-done(((bf16[8,128,512]{2,1,0:T(8,128)(2,1)}), bf16[8,128,512]{2,1,0:T(8,128)(2,1)S(1)}, u32[]{:S(2)}, u32[]{:S(2)}) %all-to-all-start.1) | async-done | bytes 1048608 | tf_op jit(solution)/shard_map/all_to_all | solution.py:203
  204.7 4.0 %gather_fusion.1 = bf16[1024,512]{1,0:T(8,128)(2,1)S(1)} fusion(bf16[1024,512]{1,0:T(8,128)(2,1)S(1)} %bitcast.91, s32[1024]{0:T(1024)S(1)} %broadcast_clamp_fusion), kind=kCustom, calls=%fused_computation.1 | custom fusion | bytes 2101248 | tf_op jit(solution)/shard_map/jit(_take)/gather | solution.py:205
  208.7 0.4 gather.12
  209.2 5.2 %multiply_reduce_fusion = bf16[512,512]{1,0:T(8,128)(2,1)} fusion(bf16[512,2,512]{2,1,0:T(2,128)(2,1)S(1)} %gather.12, pred[512,2]{1,0:T(8,128)(4,1)S(1)} %copy.43, f32[512,2]{1,0:T(8,128)S(1)} %copy.45), kind=kLoop, calls=%fused_computation.14 | loop fusion | flops 1835008 | bytes 1577984 | tf_op jit(solution)/shard_map/reduce_sum | solution.py:209
  214.4 2.0 reduce-scatter.3.cloned.1.call-done
  (84 shorter events, 4.7 us)
Async XLA Ops:
  7.2 108.0 %copy-start = (bf16[1,256,2048]{2,1,0:T(8,128)(2,1)S(1)}, bf16[1,256,2048]{2,1,0:T(8,128)(2,1)}, u32[]{:S(2)}) copy-start(bf16[1,256,2048]{2,1,0:T(8,128)(2,1)} %param.33) | copy-start | bytes 3145732
  7.2 177.7 %reduce-scatter.5.cloned.1.call-start = ((), (), s32[]{:S(2)}) async-start(), calls=%async_computation.5 | async-start | bytes 5242880 | tf_op jit(solution)/shard_map/reduce_scatter | solution.py:200
  61.4 14.2 %collective-permute-start = (bf16[1024,512]{1,0:T(8,128)(2,1)S(1)}, bf16[1024,512]{1,0:T(8,128)(2,1)S(1)}, u32[]{:S(2)}, u32[]{:S(2)}) collective-permute-start(bf16[1024,512]{1,0:T(8,128)(2,1)S(1)} %bitcast.92), channel_id=1, source_target_pairs={{0,1},{1,2},{2,3},{3,0},{4,5},{5,6},{6,7},{7,4},{8,9},{9,10},{10,1... | collective-permute-start | bytes 3145736 | tf_op jit(solution)/shard_map/ppermute | solution.py:186
  75.6 14.3 %collective-permute-start.1 = (bf16[1024,512]{1,0:T(8,128)(2,1)S(1)}, bf16[1024,512]{1,0:T(8,128)(2,1)}, u32[]{:S(2)}, u32[]{:S(2)}) collective-permute-start(bf16[1024,512]{1,0:T(8,128)(2,1)S(1)} %collective-permute-done), channel_id=1, source_target_pairs={{0,1},{1,2},{2,3},{3,0},{4,5},{5,6},{6,7},{7,4},{8,9},{9,10},{10,1... | collective-permute-start | bytes 3145736 | tf_op jit(solution)/shard_map/ppermute | solution.py:186
  89.9 14.5 %collective-permute-start.2 = (bf16[1024,512]{1,0:T(8,128)(2,1)}, bf16[1024,512]{1,0:T(8,128)(2,1)}, u32[]{:S(2)}, u32[]{:S(2)}) collective-permute-start(bf16[1024,512]{1,0:T(8,128)(2,1)} %collective-permute-done.1), channel_id=1, source_target_pairs={{0,1},{1,2},{2,3},{3,0},{4,5},{5,6},{6,7},{7,4},{8,9},{9,10},{10,1... | collective-permute-start | bytes 3145736 | tf_op jit(solution)/shard_map/ppermute | solution.py:186
  89.9 24.0 %copy-start.11 = (bf16[1,2048,256]{2,1,0:T(8,128)(2,1)S(1)}, bf16[1,2048,256]{2,1,0:T(8,128)(2,1)}, u32[]{:S(2)}) copy-start(bf16[1,2048,256]{2,1,0:T(8,128)(2,1)} %param.32) | copy-start | bytes 3145732
  110.6 3.2 %copy-start.5 = (bf16[1024,4096]{1,0:T(8,128)(2,1)}, bf16[1024,4096]{1,0:T(8,128)(2,1)S(1)}, u32[]{:S(2)}) copy-start(bf16[1024,4096]{1,0:T(8,128)(2,1)S(1)} %constant_dynamic-update-slice_fusion) | copy-start | bytes 25165828
  115.2 9.1 %copy-start.7 = (bf16[128,64]{0,1:T(8,128)(2,1)S(1)}, bf16[128,64]{0,1:T(8,128)(2,1)}, u32[]{:S(2)}) copy-start(bf16[128,64]{0,1:T(8,128)(2,1)} %param.19) | copy-start | bytes 49156
  115.2 9.1 %copy-start.2 = (bf16[128,512]{1,0:T(8,128)(2,1)S(1)}, bf16[128,512]{1,0:T(8,128)(2,1)}, u32[]{:S(2)}) copy-start(bf16[128,512]{1,0:T(8,128)(2,1)} %param.17) | copy-start | bytes 393220
  115.2 9.2 %copy-start.4 = (bf16[512,128]{1,0:T(8,128)(2,1)S(1)}, bf16[512,128]{1,0:T(8,128)(2,1)}, u32[]{:S(2)}) copy-start(bf16[512,128]{1,0:T(8,128)(2,1)} %param.23) | copy-start | bytes 393220
  115.2 9.2 %copy-start.9 = (f32[512]{0:T(512)S(1)}, f32[512]{0:T(512)}, u32[]{:S(2)}) copy-start(f32[512]{0:T(512)} %param.20) | copy-start | bytes 6148
  115.2 36.0 %copy-start.3 = (bf16[512,256]{1,0:T(8,128)(2,1)S(1)}, bf16[512,256]{1,0:T(8,128)(2,1)}, u32[]{:S(2)}) copy-start(bf16[512,256]{1,0:T(8,128)(2,1)} %param.22) | copy-start | bytes 786436
  115.2 36.2 %copy-start.6 = (bf16[128,256]{1,0:T(8,128)(2,1)S(1)}, bf16[128,256]{1,0:T(8,128)(2,1)}, u32[]{:S(2)}) copy-start(bf16[128,256]{1,0:T(8,128)(2,1)} %param.18) | copy-start | bytes 196612
  115.2 68.4 %copy-start.12 = (bf16[256,256]{1,0:T(8,128)(2,1)S(1)}, bf16[256,256]{1,0:T(8,128)(2,1)}, u32[]{:S(2)}) copy-start(bf16[256,256]{1,0:T(8,128)(2,1)} %param.24) | copy-start | bytes 393220
  115.2 68.4 %copy-start.14 = (f32[256]{0:T(256)S(1)}, f32[256]{0:T(256)}, u32[]{:S(2)}) copy-start(f32[256]{0:T(256)} %param.21) | copy-start | bytes 3076
  124.2 64.8 %copy-start.13 = (bf16[256,256]{1,0:T(8,128)(2,1)S(1)}, bf16[256,256]{1,0:T(8,128)(2,1)}, u32[]{:S(2)}) copy-start(bf16[256,256]{1,0:T(8,128)(2,1)} %param.25) | copy-start | bytes 393220
  124.2 69.4 %copy-start.8 = (s32[512,2]{0,1:T(2,128)S(1)}, s32[512,2]{0,1:T(2,128)}, u32[]{:S(2)}) copy-start(s32[512,2]{0,1:T(2,128)} %param.29) | copy-start | bytes 12292
  124.3 69.6 %copy-start.10 = (f32[512,2]{0,1:T(2,128)S(1)}, f32[512,2]{0,1:T(2,128)}, u32[]{:S(2)}) copy-start(f32[512,2]{0,1:T(2,128)} %param.30) | copy-start | bytes 12292
  183.4 1.0 copy-start.1
  184.9 19.9 %all-to-all-start.1 = ((bf16[8,128,512]{2,1,0:T(8,128)(2,1)}), bf16[8,128,512]{2,1,0:T(8,128)(2,1)S(1)}, u32[]{:S(2)}, u32[]{:S(2)}) async-start(bf16[8,128,512]{2,1,0:T(8,128)(2,1)} %bitcast.96), calls=%async_computation.3 | async-start | bytes 2097152 | tf_op jit(solution)/shard_map/all_to_all | solution.py:203
  188.4 28.0 %reduce-scatter.3.cloned.1.call-start = ((), (), s32[]{:S(2)}) async-start(), calls=%async_computation.4 | async-start | bytes 655360 | tf_op jit(solution)/shard_map/reduce_scatter | solution.py:146
Sparse Core Ops, SparseCore 0:
  124.3 43.4 reduce-scatter.4
  193.5 22.8 reduce-scatter.2
